TPU v7x, 32 devices: a whole 2x2x4 slice. The times are simulated.
32 devices in a mesh: sp: 8 (over z, core), tp: 4 (over y, x).
Axes of the slice: x: 2, y: 2, z: 4, core: 2. Of those that a mesh axis runs over, the one named last changes fastest.
Arguments:
- pool_in: bfloat16 [512, 3072], P('tp', 'sp'), may hold values from -8 to 8
- doc_ids: int32 [3072], P('sp'), may hold values from 0 to 3, never falling along the last dimension, each value on 1 to 1536 neighbouring positions
- pool_map: bfloat16 [8, 64, 64], replicated, may hold values from -0.75 to 0.75
- pool_scale: float32 [512], replicated, may hold values from 0.1 to 1.9
- w_out: bfloat16 [512, 2048], P(None, 'tp'), may hold values from -0.25 to 0.25
- gate_logit: bfloat16 [3072, 2048], P('sp', 'tp'), may hold values from -8 to 8
- residual: bfloat16 [3072, 2048], P('sp', 'tp'), may hold values from -4 to 4
- first_gain: float32 [2048], P('tp'), may hold values from 0.1 to 1.9
- first_bias: float32 [2048], P('tp'), may hold values from -1.5 to 1.5
- routes: int32 [3072, 2], P('sp'), may hold values from 0 to 7, all different within a row; in each aligned block of 384 rows (0 to 383, 384 to 767, ...) at most 192 rows name the same one
- route_weight: float32 [3072, 2], P('sp'), may hold values from 0.25 to 1
- w_gate: bfloat16 [8, 2048, 1024], P('sp', None, 'tp'), may hold values from -0.125 to 0.125
- w_up: bfloat16 [8, 2048, 1024], P('sp', None, 'tp'), may hold values from -0.125 to 0.125
- w_down: bfloat16 [8, 1024, 2048], P('sp', None, 'tp'), may hold values from -0.375 to 0.375
- second_gain: float32 [2048], P('tp'), may hold values from 0.1 to 1.9
- second_bias: float32 [2048], P('tp'), may hold values from -1.5 to 1.5
Outputs:
- layer_out: bfloat16 [3072, 2048], P('sp', 'tp')
Inputs may be any that keep to these rules, and one draw needn't show every extreme that they name: `doc_ids`: never falling; each document spans 1 to 1536 positions. `routes`: each row names 2 different experts; in each aligned block of 384 rows (the rows of one index of sp) no expert is named by more than 192 rows, a bound that some block reaches.
All inputs are finite; a program needn't handle non-finite values.
Results may differ from a plain program's by a relative error of at most 0.008.
Values may be sent and summed in bfloat16 or wider, within the bound.
A program may use at most 64 MiB of HBM per device.

v0:
```python
import functools

import jax
import jax.numpy as jnp
from jax import lax
from jax.experimental import pallas as pl
from jax.experimental.pallas import tpu as pltpu
from jax.sharding import PartitionSpec as P

GROUP_W = 64


EPS = 1e-05
ALPHA = 8.0**0.25
halo_len = 16


def shifted(shard, axis, by):
    size = lax.axis_size(axis)
    pairs = [(i, i + by) for i in range(size) if 0 <= i + by < size]
    return lax.ppermute(shard, axis, pairs)


def entering(shard, axis, combine, identity):
    size, place = (lax.axis_size(axis), lax.axis_index(axis))
    everything = jax.tree.map(lambda part: lax.all_gather(part, axis), shard)
    start = jax.tree.map(
        lambda part, zero: jnp.broadcast_to(jnp.asarray(zero, part.dtype), part.shape),
        shard,
        identity,
    )

    def turn(k, before):
        reached = k < place
        new = combine(before, jax.tree.map(lambda part: part[k], everything))
        return jax.tree.map(lambda a, b: jnp.where(reached, a, b), new, before)

    return lax.fori_loop(0, size, turn, start)


def carry_join(earlier, later):
    keeping = 1.0 - later[2]
    return (
        later[0] + keeping * earlier[0],
        later[1] + keeping * earlier[1],
        jnp.maximum(earlier[2], later[2]),
    )


def apply_norm(row_data, totals, gain_vec, bias_vec, features):
    row_mean = totals[0][:, None] / features
    row_var = totals[1][:, None] / features - row_mean * row_mean
    return (row_data - row_mean) * lax.rsqrt(row_var + EPS) * gain_vec + bias_vec


def pool_scales(pool_in, doc_ids):
    channels_dev, positions = pool_in.shape
    edge_block = jnp.concatenate(
        [
            pool_in[:, positions - halo_len :],
            doc_ids[None, positions - halo_len :].astype(jnp.bfloat16),
        ],
        axis=0,
    )
    previous = shifted(edge_block, "sp", 1)
    prior_ids = jnp.where(
        lax.axis_index("sp") == 0, -1.0, previous[channels_dev].astype(jnp.float32)
    )
    ids_ext = jnp.concatenate([prior_ids, doc_ids.astype(jnp.float32)])
    inputs_ext = jnp.concatenate([previous[:channels_dev], pool_in], axis=1).astype(jnp.float32)
    length = positions + halo_len
    opening = jnp.concatenate([jnp.zeros((1,), bool), ids_ext[1:] != ids_ext[:-1]])
    places = jnp.arange(length, dtype=jnp.int32)
    doc_start = lax.cummax(jnp.where(opening, places, 0), axis=0)
    prefix = jnp.concatenate(
        [jnp.zeros((channels_dev, 1), jnp.float32), jnp.cumsum(inputs_ext, axis=1)], axis=1
    )
    start_here = doc_start[halo_len:]
    upper_at = places[halo_len:] + 1
    at_start = jnp.take(prefix, start_here, axis=1)
    current = prefix[:, halo_len + 1 :]
    group_id = (
        lax.axis_index("tp") * channels_dev + jnp.arange(channels_dev, dtype=jnp.int32)
    ) // GROUP_W
    doc_mask = (group_id % 2 == 1)[:, None]
    window = jnp.left_shift(2, group_id // 2 % 4)[:, None]
    lagged = jnp.zeros((channels_dev, positions), jnp.float32)
    for octave in range(4):
        window_len = 2 << octave
        begin = halo_len + 1 - window_len
        lagged = lagged + jnp.where(window == window_len, prefix[:, begin : begin + positions], 0.0)
    lower_at = jnp.maximum(upper_at[None, :] - window, start_here[None, :])
    win_sum = current - jnp.where(
        start_here[None, :] > upper_at[None, :] - window, at_start, lagged
    )
    win_count = (upper_at[None, :] - lower_at).astype(jnp.float32)
    opened = start_here >= halo_len
    local_sum = current - jnp.where(opened[None, :], at_start, prefix[:, halo_len : halo_len + 1])
    local_count = (upper_at - jnp.maximum(start_here, halo_len)).astype(jnp.float32)
    last_start = doc_start[length - 1]
    last_base = jnp.where(
        last_start >= halo_len,
        lax.dynamic_slice_in_dim(prefix, last_start, 1, 1)[:, 0],
        prefix[:, halo_len],
    )
    summary = (
        prefix[:, length] - last_base,
        (length - jnp.maximum(last_start, halo_len)).astype(jnp.float32),
        (last_start >= halo_len).astype(jnp.float32),
    )
    nothing = (jnp.zeros((channels_dev,), jnp.float32), jnp.float32(0.0), jnp.float32(0.0))
    carried = entering(summary, "sp", carry_join, nothing)
    doc_sum = local_sum + jnp.where(opened[None, :], 0.0, carried[0][:, None])
    doc_count = local_count + jnp.where(opened, 0.0, carried[1])
    pooled = (
        jnp.where(doc_mask, doc_sum / doc_count[None, :], win_sum / win_count)
        - inputs_ext[:, halo_len:]
    )
    return pooled.astype(jnp.bfloat16)


def general_body(
    pool_in,
    doc_ids,
    pool_map,
    pool_scale,
    w_out,
    gate_logit,
    residual,
    first_gain,
    first_bias,
    routes,
    route_weight,
    w_gate,
    w_up,
    w_down,
    second_gain,
    second_bias,
):
    pooled = pool_scales(pool_in, doc_ids)
    positions = pool_in.shape[1]
    features = residual.shape[1] * lax.axis_size("tp")
    gathered = lax.all_gather(pooled, "tp", axis=0, tiled=True)
    group_count = gathered.shape[0] // GROUP_W
    grouped = jnp.einsum(
        "gct,gcd->tgd",
        gathered.reshape(group_count, GROUP_W, positions),
        pool_map,
        preferred_element_type=jnp.float32,
    )
    mapped = (grouped.reshape(positions, group_count * GROUP_W) * pool_scale).astype(jnp.bfloat16)
    mixer_out = jnp.dot(mapped, w_out, preferred_element_type=jnp.float32) * jax.nn.sigmoid(
        gate_logit.astype(jnp.float32)
    )
    mixed_rows = ALPHA * residual.astype(jnp.float32) + mixer_out
    first_totals = lax.psum(
        (jnp.sum(mixed_rows, axis=1), jnp.sum(mixed_rows * mixed_rows, axis=1)), "tp"
    )
    normed = apply_norm(mixed_rows, first_totals, first_gain, first_bias, features).astype(
        jnp.bfloat16
    )
    experts = lax.axis_size("sp")
    pairs = routes.shape[1]
    slots_per = 2 * positions * pairs // experts
    flat_routes = routes.reshape(-1)
    one_hot = (flat_routes[:, None] == jnp.arange(experts, dtype=jnp.int32)[None, :]).astype(
        jnp.int32
    )
    slot_rank = jnp.sum((jnp.cumsum(one_hot, axis=0, dtype=jnp.int32) - 1) * one_hot, axis=1)
    slot_ids = flat_routes * slots_per + slot_rank
    token_of = jnp.arange(flat_routes.shape[0], dtype=jnp.int32) // pairs
    outgoing = (
        jnp.zeros((experts * slots_per, normed.shape[1]), jnp.bfloat16)
        .at[slot_ids]
        .set(normed[token_of])
    )
    arrived = lax.all_to_all(outgoing, "sp", split_axis=0, concat_axis=0, tiled=True)
    inputs = lax.all_gather(arrived, "tp", axis=1, tiled=True)
    gate_part = jnp.dot(inputs, w_gate[0], preferred_element_type=jnp.float32)
    up_part = jnp.dot(inputs, w_up[0], preferred_element_type=jnp.float32)
    hidden = (jax.nn.silu(gate_part) * up_part).astype(jnp.bfloat16)
    down_part = w_down[0]
    result = jnp.dot(
        lax.all_gather(hidden, "tp", axis=1, tiled=True),
        down_part,
        preferred_element_type=jnp.float32,
    )
    returned = lax.all_to_all(
        result.astype(jnp.bfloat16), "sp", split_axis=0, concat_axis=0, tiled=True
    )
    picked = returned[slot_ids].astype(jnp.float32).reshape(positions, pairs, returned.shape[1])
    moe_sum = jnp.sum(picked * route_weight[:, :, None], axis=1)
    final_rows = ALPHA * normed.astype(jnp.float32) + moe_sum
    second_totals = lax.psum(
        (jnp.sum(final_rows, axis=1), jnp.sum(final_rows * final_rows, axis=1)), "tp"
    )
    return apply_norm(final_rows, second_totals, second_gain, second_bias, features).astype(
        jnp.bfloat16
    )


NT = (((1,), (1,)), ((), ()))
F32 = jnp.float32
BF16 = jnp.bfloat16
LANES = 128


def dot_nt(a, b):
    return lax.dot_general(a, b, NT, preferred_element_type=F32)


def dot_nn(a, b):
    return jnp.dot(a, b, preferred_element_type=F32)


def enter(n_sp, n_tp):
    sp, tp = lax.axis_index("sp"), lax.axis_index("tp")
    barrier = pltpu.get_barrier_semaphore()
    for d in range(1, n_sp):
        pl.semaphore_signal(barrier, inc=1, device_id={"sp": lax.rem(sp + d, n_sp)})
    for d in range(1, n_tp):
        pl.semaphore_signal(barrier, inc=1, device_id={"tp": lax.rem(tp + d, n_tp)})
    pl.semaphore_wait(barrier, n_sp + n_tp - 2)


def remote(src, dst, send, recv, axis, peer):
    return pltpu.make_async_remote_copy(
        src_ref=src, dst_ref=dst, send_sem=send, recv_sem=recv, device_id={axis: peer}
    )


def share(buf, axis, n, send, recv):
    me = lax.axis_index(axis)
    for d in range(1, n):
        remote(
            buf.at[me], buf.at[me], send.at[d], recv.at[me], axis, lax.rem(me + d, n)
        ).start()


def collect(buf, axis, n, send, recv):
    me = lax.axis_index(axis)
    for d in range(1, n):
        other = lax.rem(me + d, n)
        remote(buf.at[other], buf.at[other], send.at[d], recv.at[other], axis, other).wait_recv()


def settle(buf, axis, n, send, recv):
    me = lax.axis_index(axis)
    for d in range(1, n):
        remote(
            buf.at[me], buf.at[me], send.at[d], recv.at[me], axis, lax.rem(me + d, n)
        ).wait_send()


def row_totals(rows, stats, n_tp, send, recv):
    me = lax.axis_index("tp")
    lane = lax.broadcasted_iota(jnp.int32, (rows.shape[0], LANES), 1)
    first = jnp.sum(rows, axis=1, keepdims=True)
    second = jnp.sum(rows * rows, axis=1, keepdims=True)
    both = jnp.where(lane == 0, first, jnp.where(lane == 1, second, 0.0))
    stats[me] = jnp.transpose(both)[:8]
    share(stats, "tp", n_tp, send, recv)
    collect(stats, "tp", n_tp, send, recv)
    total = stats[0]
    for k in range(1, n_tp):
        total = total + stats[k]
    total = jnp.concatenate([total, jnp.zeros((LANES - 8, total.shape[1]), F32)], axis=0)
    columns = jnp.transpose(total)
    return columns[:, 0:1], columns[:, 1:2]


def normalise(rows, totals, gain, bias, features):
    mean = totals[0] / features
    var = totals[1] / features - mean * mean
    return (rows - mean) * lax.rsqrt(var + EPS) * gain + bias


def near_peers():
    tp = lax.axis_index("tp")
    beside = tp + 1 - 2 * lax.rem(tp, 2)
    return beside, lax.rem(tp + 2, 4), lax.rem(beside + 2, 4)


def near_copies(buf, send, recv):
    tp = lax.axis_index("tp")
    beside, below, _ = near_peers()
    return [
        remote(buf.at[tp], buf.at[tp], send.at[0], recv.at[0], "tp", beside),
        remote(buf.at[tp], buf.at[tp], send.at[1], recv.at[1], "tp", below),
    ]


def relay_copies(buf, send, recv):
    beside, below, _ = near_peers()
    half = buf.shape[1] // 2
    upper, lower = buf.at[beside, :half], buf.at[below, half:]
    return [
        remote(upper, upper, send.at[2], recv.at[2], "tp", below),
        remote(lower, lower, send.at[3], recv.at[3], "tp", beside),
    ]


def relay(buf, send, recv):
    beside, below, _ = near_peers()
    onward = relay_copies(buf, send, recv)
    remote(buf.at[beside], buf.at[beside], send.at[0], recv.at[0], "tp", beside).wait_recv()
    onward[0].start()
    remote(buf.at[below], buf.at[below], send.at[1], recv.at[1], "tp", below).wait_recv()
    onward[1].start()


def far_arrived(buf, send, recv):
    beside, below, far = near_peers()
    half = buf.shape[1] // 2
    upper, lower = buf.at[far, :half], buf.at[far, half:]
    remote(upper, upper, send.at[2], recv.at[2], "tp", below).wait_recv()
    remote(lower, lower, send.at[3], recv.at[3], "tp", beside).wait_recv()


def layer_kernel(
    n_sp, n_tp, pool, doc_row, route_row, weight_row, pool_map, scale, gain, bias, gain2, bias2,
    w_out_hbm, gate_hbm, residual_hbm, w_gate_hbm, w_up_hbm, w_down_hbm, out,
    w_out, gate, residual, w_gate, w_up, w_down,
    halo, halo_ids, tails, mapped, stats, stats2, normed,
    packed, arrived, hidden, result, back, load_sem,
    halo_send, halo_recv, tail_send, tail_recv, map_send, map_recv, stat_send, stat_recv,
    z_send, z_recv, x_send, x_recv, h_send, h_recv, r_send, r_recv, stat2_send, stat2_recv,
):
    sp, tp = lax.axis_index("sp"), lax.axis_index("tp")
    channels, positions = pool.shape
    part = residual.shape[1]
    slots = packed.shape[1]
    features = part * n_tp
    loads = [
        pltpu.make_async_copy(src, dst, load_sem.at[i])
        for i, (src, dst) in enumerate([
            (w_out_hbm, w_out), (gate_hbm, gate), (residual_hbm, residual),
            (w_gate_hbm, w_gate), (w_up_hbm, w_up), (w_down_hbm, w_down),
        ])
    ]
    for load in loads:
        load.start()
    enter(n_sp, n_tp)
    after = lax.rem(sp + 1, n_sp)
    last = pl.ds(positions - LANES, LANES)
    edge = remote(pool.at[:, last], halo, halo_send.at[0], halo_recv.at[0], "sp", after)
    edge_ids = remote(doc_row.at[:, last], halo_ids, halo_send.at[1], halo_recv.at[1], "sp", after)
    edge.start()
    edge_ids.start()
    ids = doc_row[...].astype(F32)
    in_last = (ids == ids[:, positions - 1 :]).astype(F32)
    tail = dot_nt(jnp.broadcast_to(in_last, (8, positions)).astype(BF16), pool[...])
    kind = lax.broadcasted_iota(jnp.int32, tail.shape, 0)
    tail = jnp.where(kind == 1, jnp.sum(in_last, axis=1, keepdims=True), tail)
    tails[sp] = jnp.where(kind == 2, ids[:, positions - 1 :], tail)
    share(tails, "sp", n_sp, tail_send, tail_recv)
    kind = lax.broadcasted_iota(jnp.int32, (LANES, positions), 0)
    table = jnp.where(kind == 0, ids, 0.0)
    for i, row in enumerate(
        (route_row[0:1].astype(F32), route_row[1:2].astype(F32), weight_row[0:1], weight_row[1:2])
    ):
        table = jnp.where(kind == i + 1, row, table)
    columns = jnp.transpose(table)
    col = columns[:, 0:1]
    later = lax.broadcasted_iota(jnp.int32, (positions, positions), 1)
    earlier = lax.broadcasted_iota(jnp.int32, (positions, positions), 0)
    ahead = (earlier < later).astype(F32).astype(BF16)
    r0, r1 = route_row[0:1], route_row[1:2]
    named = ((r0 == kind) | (r1 == kind)).astype(F32).astype(BF16)
    rank = dot_nn(named, ahead) + (kind * slots).astype(F32)
    slot0 = jnp.sum(jnp.where(r0 == kind, rank, 0.0), axis=0, keepdims=True).astype(jnp.int32)
    slot1 = jnp.sum(jnp.where(r1 == kind, rank, 0.0), axis=0, keepdims=True).astype(jnp.int32)
    place = lax.broadcasted_iota(jnp.int32, (positions, LANES + positions), 1) - LANES
    delta = lax.broadcasted_iota(jnp.int32, (positions, LANES + positions), 0) - place
    edge.wait_recv()
    edge_ids.wait_recv()
    ext = jnp.concatenate([halo[...], pool[...]], axis=1)
    before = jnp.where(sp == 0, -1.0, halo_ids[...].astype(F32))
    ext_ids = jnp.concatenate([before, ids], axis=1)
    together = (col == ext_ids) & (delta >= 0)
    own = (delta == 0).astype(F32).astype(BF16)
    values = dot_nt(own, ext)
    sums, counts, wholes = [], [], []
    per = channels // GROUP_W
    for i in range(per):
        group = tp * per + i
        whole = lax.rem(group, 2) == 1
        window = jnp.left_shift(2, lax.rem(group // 2, 4))
        reach = jnp.where(whole, positions, window)
        least = jnp.where(whole, 0, -LANES)
        mask = (together & (delta < reach) & (place >= least)).astype(F32)
        sums.append(dot_nt(mask.astype(BF16), ext[i * GROUP_W : (i + 1) * GROUP_W]))
        counts.append(jnp.sum(mask, axis=1, keepdims=True))
        wholes.append(whole)
    collect(tails, "sp", n_sp, tail_send, tail_recv)
    opening = col[0:1]
    carry = jnp.zeros((1, channels), F32)
    carry_count = jnp.zeros((1, channels), F32)
    for k in range(n_sp - 1):
        block = tails[k]
        joins = (block[2:3] == opening) & (k < sp)
        carry = carry + jnp.where(joins, block[0:1], 0.0)
        carry_count = carry_count + jnp.where(joins, block[1:2], 0.0)
    goes_on = (col == opening).astype(F32)
    for i in range(per):
        group = tp * per + i
        span = slice(i * GROUP_W, (i + 1) * GROUP_W)
        joined = jnp.where(wholes[i], goes_on, 0.0)
        total = sums[i] + joined * carry[:, span]
        count = counts[i] + joined * carry_count[:, span]
        pooled = (total / count - values[:, span]).astype(BF16)
        factor = scale[:, pl.ds(pl.multiple_of(tp * channels, LANES), channels)][:, span]
        mapped[tp, :, span] = (dot_nn(pooled, pool_map[group]) * factor).astype(BF16)
    share(mapped, "tp", n_tp, map_send, map_recv)
    for load in loads[:3]:
        load.wait()
    opened = jax.nn.sigmoid(gate[...].astype(F32))
    kept = ALPHA * residual[...].astype(F32)
    collect(mapped, "tp", n_tp, map_send, map_recv)
    every = jnp.concatenate([mapped[k] for k in range(n_tp)], axis=1)
    rows = kept + dot_nn(every, w_out[...]) * opened
    totals = row_totals(rows, stats, n_tp, stat_send, stat_recv)
    normed[...] = normalise(rows, totals, gain[...], bias[...], features).astype(BF16)

    def pack(to):
        line = lax.broadcasted_iota(jnp.int32, (slots, positions), 0) + to * slots
        pick = ((line == slot0) | (line == slot1)).astype(F32).astype(BF16)
        return dot_nn(pick, normed[...]).astype(BF16)

    arrived[sp, tp] = pack(sp)
    for copy in near_copies(arrived.at[sp], x_send.at[sp], x_recv.at[sp]):
        copy.start()
    for k in range(1, n_sp):
        to = lax.rem(sp + n_sp - k, n_sp)
        packed[to] = pack(to)
        remote(packed.at[to], arrived.at[sp, tp], z_send.at[to], z_recv.at[sp], "sp", to).start()
    for load in loads[3:]:
        load.wait()

    def step(i, _):
        def stage(lag):
            return (i >= lag) & (i < n_sp + lag), lax.rem(sp + i + n_sp - lag, n_sp)

        live, s = stage(0)

        @pl.when(live & (i > 0))
        def _():
            remote(
                packed.at[s], arrived.at[s, tp], z_send.at[s], z_recv.at[s], "sp", s
            ).wait_recv()
            for copy in near_copies(arrived.at[s], x_send.at[s], x_recv.at[s]):
                copy.start()

        live1, s1 = stage(1)

        @pl.when(live1)
        def _():
            relay(arrived.at[s1], x_send.at[s1], x_recv.at[s1])

        live3, s3 = stage(3)

        @pl.when(live3)
        def _():
            relay(hidden.at[s3], h_send.at[s3], h_recv.at[s3])

        live2, s2 = stage(2)

        @pl.when(live2)
        def _():
            far_arrived(arrived.at[s2], x_send.at[s2], x_recv.at[s2])
            rows = jnp.concatenate([arrived[s2, k] for k in range(n_tp)], axis=1)
            gated = dot_nn(rows, w_gate[...])
            up = dot_nn(rows, w_up[...])
            hidden[s2, tp] = (gated * jax.nn.sigmoid(gated) * up).astype(BF16)
            for copy in near_copies(hidden.at[s2], h_send.at[s2], h_recv.at[s2]):
                copy.start()

        live4, s4 = stage(4)

        @pl.when(live4)
        def _():
            far_arrived(hidden.at[s4], h_send.at[s4], h_recv.at[s4])
            rows = jnp.concatenate([hidden[s4, k] for k in range(n_tp)], axis=1)
            block = dot_nn(rows, w_down[...]).astype(BF16)

            @pl.when(i == 4)
            def _():
                back[sp] = block

            @pl.when(i > 4)
            def _():
                result[s4] = block
                remote(
                    result.at[s4], back.at[sp], r_send.at[s4], r_recv.at[sp], "sp", s4
                ).start()

        return 0

    lax.fori_loop(0, n_sp + 4, step, 0)
    lane = lax.broadcasted_iota(jnp.int32, (positions, LANES), 1)
    behind = (later < earlier).astype(F32).astype(BF16)
    c0, c1 = columns[:, 1:2].astype(jnp.int32), columns[:, 2:3].astype(jnp.int32)
    named = ((c0 == lane) | (c1 == lane)).astype(F32).astype(BF16)
    rank = dot_nn(behind, named) + (lane * slots).astype(F32)
    at0 = jnp.sum(jnp.where(c0 == lane, rank, 0.0), axis=1, keepdims=True).astype(jnp.int32)
    at1 = jnp.sum(jnp.where(c1 == lane, rank, 0.0), axis=1, keepdims=True).astype(jnp.int32)
    spot = lax.broadcasted_iota(jnp.int32, (positions, n_sp * slots), 1)
    take0 = (spot == at0).astype(F32).astype(BF16)
    take1 = (spot == at1).astype(F32).astype(BF16)
    for k in range(1, n_sp):
        s = lax.rem(sp + k, n_sp)
        remote(result.at[s], back.at[s], r_send.at[s], r_recv.at[s], "sp", s).wait_recv()
    returned = back[...].reshape(n_sp * slots, part)
    moe = columns[:, 3:4] * dot_nn(take0, returned) + columns[:, 4:5] * dot_nn(take1, returned)
    rows = ALPHA * normed[...].astype(F32) + moe
    totals = row_totals(rows, stats2, n_tp, stat2_send, stat2_recv)
    out[...] = normalise(rows, totals, gain2[...], bias2[...], features).astype(BF16)

    def drain(i, _):
        s = lax.rem(sp + i, n_sp)

        @pl.when(i > 0)
        def _():
            remote(packed.at[s], arrived.at[sp, tp], z_send.at[s], z_recv.at[sp], "sp", s).wait_send()
            remote(result.at[s], back.at[sp], r_send.at[s], r_recv.at[sp], "sp", s).wait_send()

        for buf, send, recv in ((arrived, x_send, x_recv), (hidden, h_send, h_recv)):
            place = (buf.at[s], send.at[s], recv.at[s])
            for copy in near_copies(*place) + relay_copies(*place):
                copy.wait_send()
        return 0

    lax.fori_loop(0, n_sp, drain, 0)
    edge.wait_send()
    edge_ids.wait_send()
    settle(tails, "sp", n_sp, tail_send, tail_recv)
    settle(mapped, "tp", n_tp, map_send, map_recv)
    settle(stats, "tp", n_tp, stat_send, stat_recv)
    settle(stats2, "tp", n_tp, stat2_send, stat2_recv)


def body(n_sp, n_tp, *args):
    (pool_in, doc_ids, pool_map, pool_scale, w_out, gate_logit, residual, first_gain, first_bias,
     routes, route_weight, w_gate, w_up, w_down, second_gain, second_bias) = args
    channels, positions = pool_in.shape
    part = residual.shape[1]
    pairs = routes.shape[1]
    small = n_sp <= 16 and n_tp == 4 and pairs == 2
    if not small or channels % LANES or positions % LANES or part % LANES:
        return general_body(*args)
    dma = pltpu.SemaphoreType.DMA
    slots = 2 * positions * pairs // n_sp
    units = w_gate.shape[2]
    loaded = (w_out, gate_logit, residual, w_gate[0], w_up[0], w_down[0])
    vmem = pl.BlockSpec(memory_space=pltpu.VMEM)
    any_space = pl.BlockSpec(memory_space=pl.ANY)
    return pl.pallas_call(
        functools.partial(layer_kernel, n_sp, n_tp),
        out_shape=jax.ShapeDtypeStruct(residual.shape, BF16),
        in_specs=[vmem] * 10 + [any_space] * len(loaded),
        out_specs=vmem,
        scratch_shapes=[
            *(pltpu.VMEM(x.shape, x.dtype) for x in loaded),
            pltpu.VMEM((channels, LANES), BF16),
            pltpu.VMEM((1, LANES), jnp.int32),
            pltpu.VMEM((n_sp, 8, channels), F32),
            pltpu.VMEM((n_tp, positions, channels), BF16),
            pltpu.VMEM((n_tp, 8, positions), F32),
            pltpu.VMEM((n_tp, 8, positions), F32),
            pltpu.VMEM((positions, part), BF16),
            pltpu.VMEM((n_sp, slots, part), BF16),
            pltpu.VMEM((n_sp, n_tp, slots, part), BF16),
            pltpu.VMEM((n_sp, n_tp, slots, units), BF16),
            pltpu.VMEM((n_sp, slots, part), BF16),
            pltpu.VMEM((n_sp, slots, part), BF16),
            dma((len(loaded),)),
            dma((2,)), dma((2,)), dma((n_sp,)), dma((n_sp,)),
            dma((n_tp,)), dma((n_tp,)), dma((n_tp,)), dma((n_tp,)),
            dma((n_sp,)), dma((n_sp,)), dma((n_sp, 4)), dma((n_sp, 4)),
            dma((n_sp, 4)), dma((n_sp, 4)), dma((n_sp,)), dma((n_sp,)),
            dma((n_tp,)), dma((n_tp,)),
        ],
        compiler_params=pltpu.CompilerParams(
            collective_id=0, has_side_effects=True, vmem_limit_bytes=60 << 20
        ),
    )(
        pool_in, doc_ids[None], routes.T, route_weight.T, pool_map, pool_scale[None],
        first_gain[None], first_bias[None], second_gain[None], second_bias[None], *loaded,
    )


def solution(mesh):
    return jax.shard_map(
        functools.partial(body, mesh.shape["sp"], mesh.shape["tp"]),
        mesh=mesh,
        in_specs=(
            P("tp", "sp"),
            P("sp"),
            P(),
            P(),
            P(None, "tp"),
            P("sp", "tp"),
            P("sp", "tp"),
            P("tp"),
            P("tp"),
            P("sp", None),
            P("sp", None),
            P("sp", None, "tp"),
            P("sp", None, "tp"),
            P("sp", None, "tp"),
            P("tp"),
            P("tp"),
        ),
        out_specs=P("sp", "tp"),
        check_vma=False,
    )
```

profile of v0, /device:TPU:25, one launch (start us, length us, event | category | flops | bytes accessed | tf_op | source)
XLA Modules:
  0.0 127.0 jit_solution(14721852991139402164)
XLA Ops:
  0.0 0.0 copy-start
  0.0 0.7 copy-done
  0.7 0.6 broadcast_in_dim.18.doc_row
  1.2 123.9 %shard_map.154 = bf16[384,512]{1,0:T(8,128)(2,1)} custom-call(bf16[128,384]{1,0:T(8,128)(2,1)} %pool.1, s32[1,384]{1,0:T(1,128)} %broadcast_in_dim.18.doc_row, s32[2,384]{1,0:T(2,128)} %bitcast.13, f32[2,384]{1,0:T(2,128)} %bitcast.14, bf16[8,64,64]{2,1,0:T(8,128)(2,1)} %pool_map.1, f32[1,512]{1,0:T(1,128)} %bitcast.15, f32[1,512]{1,0:T(1,128)} %bitcast.16, ...), custom_call_target="tpu_custom_call" | custom-call | tf_op jit(solution)/shard_map/pallas_call | solution.py:557
  125.2 1.8 %copy.18 = bf16[384,512]{1,0:T(8,128)(2,1)} copy(bf16[384,512]{1,0:T(8,128)(2,1)} %shard_map.154) | data formatting | bytes 786432
Async XLA Ops:
  0.0 0.7 copy-start
where the time goes:
time: 127 us
  Pallas kernels  124 us (98%)
  local copies, waits for them, and re-layouts  3.01 us (2%)
    pallas_call x1, Pallas kernels, body(): pl.pallas_call(functools.partial(layer_kernel, n_sp, n_tp), out_shape=jax...  124 us

commit v1 on v0

--- a/solution.py
+++ b/solution.py
@@ -213,20 +213,42 @@
     return jnp.dot(a, b, preferred_element_type=F32)
 
 
-def enter(n_sp, n_tp):
+def layout():
     sp, tp = lax.axis_index("sp"), lax.axis_index("tp")
+    plane, core = sp // 2, lax.rem(sp, 2)
+    y, x = tp // 2, lax.rem(tp, 2)
+    return plane, core, y, x
+
+
+def near_peers():
+    tp = lax.axis_index("tp")
+    beside = tp + 1 - 2 * lax.rem(tp, 2)
+    return beside, lax.rem(tp + 2, 4), lax.rem(beside + 2, 4)
+
+
+def enter(n_sp):
+    sp = lax.axis_index("sp")
+    beside, below, far = near_peers()
     barrier = pltpu.get_barrier_semaphore()
-    for d in range(1, n_sp):
-        pl.semaphore_signal(barrier, inc=1, device_id={"sp": lax.rem(sp + d, n_sp)})
-    for d in range(1, n_tp):
-        pl.semaphore_signal(barrier, inc=1, device_id={"tp": lax.rem(tp + d, n_tp)})
-    pl.semaphore_wait(barrier, n_sp + n_tp - 2)
+    for d in range(n_sp):
+        if d:
+            pl.semaphore_signal(barrier, inc=1, device_id={"sp": lax.rem(sp + d, n_sp)})
+        pl.semaphore_signal(
+            barrier, inc=1, device_id={"sp": lax.rem(sp + d, n_sp), "tp": beside}
+        )
+    for peer in (below, far):
+        pl.semaphore_signal(barrier, inc=1, device_id={"tp": peer})
+    pl.semaphore_wait(barrier, 2 * n_sp + 1)
+
+
+def remote_to(src, dst, send, recv, device):
+    return pltpu.make_async_remote_copy(
+        src_ref=src, dst_ref=dst, send_sem=send, recv_sem=recv, device_id=device
+    )
 
 
 def remote(src, dst, send, recv, axis, peer):
-    return pltpu.make_async_remote_copy(
-        src_ref=src, dst_ref=dst, send_sem=send, recv_sem=recv, device_id={axis: peer}
-    )
+    return remote_to(src, dst, send, recv, {axis: peer})
 
 
 def share(buf, axis, n, send, recv):
@@ -275,78 +297,86 @@
     return (rows - mean) * lax.rsqrt(var + EPS) * gain + bias
 
 
-def near_peers():
-    tp = lax.axis_index("tp")
-    beside = tp + 1 - 2 * lax.rem(tp, 2)
-    return beside, lax.rem(tp + 2, 4), lax.rem(beside + 2, 4)
-
-
-def near_copies(buf, send, recv):
-    tp = lax.axis_index("tp")
-    beside, below, _ = near_peers()
-    return [
-        remote(buf.at[tp], buf.at[tp], send.at[0], recv.at[0], "tp", beside),
-        remote(buf.at[tp], buf.at[tp], send.at[1], recv.at[1], "tp", below),
-    ]
-
-
-def relay_copies(buf, send, recv):
-    beside, below, _ = near_peers()
-    half = buf.shape[1] // 2
-    upper, lower = buf.at[beside, :half], buf.at[below, half:]
-    return [
-        remote(upper, upper, send.at[2], recv.at[2], "tp", below),
-        remote(lower, lower, send.at[3], recv.at[3], "tp", beside),
-    ]
-
-
-def relay(buf, send, recv):
-    beside, below, _ = near_peers()
-    onward = relay_copies(buf, send, recv)
-    remote(buf.at[beside], buf.at[beside], send.at[0], recv.at[0], "tp", beside).wait_recv()
-    onward[0].start()
-    remote(buf.at[below], buf.at[below], send.at[1], recv.at[1], "tp", below).wait_recv()
-    onward[1].start()
-
-
-def far_arrived(buf, send, recv):
-    beside, below, far = near_peers()
-    half = buf.shape[1] // 2
-    upper, lower = buf.at[far, :half], buf.at[far, half:]
-    remote(upper, upper, send.at[2], recv.at[2], "tp", below).wait_recv()
-    remote(lower, lower, send.at[3], recv.at[3], "tp", beside).wait_recv()
-
-
 def layer_kernel(
     n_sp, n_tp, pool, doc_row, route_row, weight_row, pool_map, scale, gain, bias, gain2, bias2,
     w_out_hbm, gate_hbm, residual_hbm, w_gate_hbm, w_up_hbm, w_down_hbm, out,
     w_out, gate, residual, w_gate, w_up, w_down,
-    halo, halo_ids, tails, mapped, stats, stats2, normed,
-    packed, arrived, hidden, result, back, load_sem,
+    halo, halo_ids, tails, mapped, stats, stats2, tables, blocks,
+    aside, inputs, hidden, result, back, load_sem, w_send, w_recv,
     halo_send, halo_recv, tail_send, tail_recv, map_send, map_recv, stat_send, stat_recv,
-    z_send, z_recv, x_send, x_recv, h_send, h_recv, r_send, r_recv, stat2_send, stat2_recv,
+    t_send, t_recv, z_send, z_recv, a_send, a_recv, y_send, y_recv, d_send, d_recv,
+    h_send, h_recv, r_send, r_recv, stat2_send, stat2_recv,
 ):
     sp, tp = lax.axis_index("sp"), lax.axis_index("tp")
+    plane, core, y, x = layout()
+    partner = sp + 1 - 2 * core
+    beside, below, far = near_peers()
+    n_z = n_sp // 2
+    steps = 2 * n_z
     channels, positions = pool.shape
     part = residual.shape[1]
-    slots = packed.shape[1]
+    half = aside.shape[1]
+    slots = 2 * half
     features = part * n_tp
+    toward = 1 - 2 * (plane // (n_z // 2))
+    straight = x == core
+    expert = 2 * plane + x
     loads = [
         pltpu.make_async_copy(src, dst, load_sem.at[i])
         for i, (src, dst) in enumerate([
             (w_out_hbm, w_out), (gate_hbm, gate), (residual_hbm, residual),
-            (w_gate_hbm, w_gate), (w_up_hbm, w_up), (w_down_hbm, w_down),
         ])
     ]
     for load in loads:
         load.start()
-    enter(n_sp, n_tp)
+    pieces = []
+    for pair, cuts in ((((w_gate_hbm, w_gate), (w_up_hbm, w_up)), 4), (((w_down_hbm, w_down),), 4)):
+        for cut in range(cuts):
+            for src, dst in pair:
+                size = dst.shape[0] // cuts
+                span = pl.ds(cut * size, size)
+                pieces.append((src.at[span], dst.at[span]))
+    crossing = [
+        remote_to(
+            src, dst, w_send.at[i], w_recv.at[i],
+            {"sp": 2 * plane + x, "tp": 2 * y + core},
+        )
+        for i, (src, dst) in enumerate(pieces)
+    ]
+    staying = [
+        pltpu.make_async_copy(src, dst, w_recv.at[i]) for i, (src, dst) in enumerate(pieces)
+    ]
+
+    @pl.when(straight)
+    def _():
+        for copy in staying:
+            copy.start()
+
+    def cross(first, last):
+        @pl.when(jnp.logical_not(straight))
+        def _():
+            for copy in crossing[first:last]:
+                copy.start()
+
+    def weights_here(first, last):
+        @pl.when(straight)
+        def _():
+            for copy in staying[first:last]:
+                copy.wait()
+
+        @pl.when(jnp.logical_not(straight))
+        def _():
+            for copy in crossing[first:last]:
+                copy.wait_recv()
+
+    enter(n_sp)
     after = lax.rem(sp + 1, n_sp)
     last = pl.ds(positions - LANES, LANES)
     edge = remote(pool.at[:, last], halo, halo_send.at[0], halo_recv.at[0], "sp", after)
     edge_ids = remote(doc_row.at[:, last], halo_ids, halo_send.at[1], halo_recv.at[1], "sp", after)
     edge.start()
     edge_ids.start()
+    cross(0, 3)
     ids = doc_row[...].astype(F32)
     in_last = (ids == ids[:, positions - 1 :]).astype(F32)
     tail = dot_nt(jnp.broadcast_to(in_last, (8, positions)).astype(BF16), pool[...])
@@ -355,21 +385,29 @@
     tails[sp] = jnp.where(kind == 2, ids[:, positions - 1 :], tail)
     share(tails, "sp", n_sp, tail_send, tail_recv)
     kind = lax.broadcasted_iota(jnp.int32, (LANES, positions), 0)
-    table = jnp.where(kind == 0, ids, 0.0)
-    for i, row in enumerate(
-        (route_row[0:1].astype(F32), route_row[1:2].astype(F32), weight_row[0:1], weight_row[1:2])
-    ):
-        table = jnp.where(kind == i + 1, row, table)
-    columns = jnp.transpose(table)
-    col = columns[:, 0:1]
     later = lax.broadcasted_iota(jnp.int32, (positions, positions), 1)
     earlier = lax.broadcasted_iota(jnp.int32, (positions, positions), 0)
     ahead = (earlier < later).astype(F32).astype(BF16)
     r0, r1 = route_row[0:1], route_row[1:2]
     named = ((r0 == kind) | (r1 == kind)).astype(F32).astype(BF16)
     rank = dot_nn(named, ahead) + (kind * slots).astype(F32)
-    slot0 = jnp.sum(jnp.where(r0 == kind, rank, 0.0), axis=0, keepdims=True).astype(jnp.int32)
-    slot1 = jnp.sum(jnp.where(r1 == kind, rank, 0.0), axis=0, keepdims=True).astype(jnp.int32)
+    slot0 = jnp.sum(jnp.where(r0 == kind, rank, 0.0), axis=0, keepdims=True)
+    slot1 = jnp.sum(jnp.where(r1 == kind, rank, 0.0), axis=0, keepdims=True)
+    table = jnp.where(kind == 0, slot0, jnp.where(kind == 1, slot1, 0.0))
+    for i, row in enumerate((ids, weight_row[0:1], weight_row[1:2])):
+        table = jnp.where(kind == i + 2, row, table)
+    tables[plane] = table[:8]
+
+    def table_copy(d):
+        to = lax.rem(plane + d, n_z)
+        return remote(
+            tables.at[plane], tables.at[plane], t_send.at[d], t_recv.at[plane], "sp", 2 * to + core
+        )
+
+    for d in range(1, n_z):
+        table_copy(d).start()
+    columns = jnp.transpose(table)
+    col = columns[:, 2:3]
     place = lax.broadcasted_iota(jnp.int32, (positions, LANES + positions), 1) - LANES
     delta = lax.broadcasted_iota(jnp.int32, (positions, LANES + positions), 0) - place
     edge.wait_recv()
@@ -412,7 +450,8 @@
         factor = scale[:, pl.ds(pl.multiple_of(tp * channels, LANES), channels)][:, span]
         mapped[tp, :, span] = (dot_nn(pooled, pool_map[group]) * factor).astype(BF16)
     share(mapped, "tp", n_tp, map_send, map_recv)
-    for load in loads[:3]:
+    cross(3, 5)
+    for load in loads:
         load.wait()
     opened = jax.nn.sigmoid(gate[...].astype(F32))
     kept = ALPHA * residual[...].astype(F32)
@@ -420,117 +459,258 @@
     every = jnp.concatenate([mapped[k] for k in range(n_tp)], axis=1)
     rows = kept + dot_nn(every, w_out[...]) * opened
     totals = row_totals(rows, stats, n_tp, stat_send, stat_recv)
-    normed[...] = normalise(rows, totals, gain[...], bias[...], features).astype(BF16)
-
-    def pack(to):
-        line = lax.broadcasted_iota(jnp.int32, (slots, positions), 0) + to * slots
-        pick = ((line == slot0) | (line == slot1)).astype(F32).astype(BF16)
-        return dot_nn(pick, normed[...]).astype(BF16)
-
-    arrived[sp, tp] = pack(sp)
-    for copy in near_copies(arrived.at[sp], x_send.at[sp], x_recv.at[sp]):
-        copy.start()
-    for k in range(1, n_sp):
-        to = lax.rem(sp + n_sp - k, n_sp)
-        packed[to] = pack(to)
-        remote(packed.at[to], arrived.at[sp, tp], z_send.at[to], z_recv.at[sp], "sp", to).start()
-    for load in loads[3:]:
-        load.wait()
-
-    def step(i, _):
-        def stage(lag):
-            return (i >= lag) & (i < n_sp + lag), lax.rem(sp + i + n_sp - lag, n_sp)
-
-        live, s = stage(0)
-
-        @pl.when(live & (i > 0))
-        def _():
-            remote(
-                packed.at[s], arrived.at[s, tp], z_send.at[s], z_recv.at[s], "sp", s
-            ).wait_recv()
-            for copy in near_copies(arrived.at[s], x_send.at[s], x_recv.at[s]):
-                copy.start()
-
-        live1, s1 = stage(1)
-
-        @pl.when(live1)
-        def _():
-            relay(arrived.at[s1], x_send.at[s1], x_recv.at[s1])
-
-        live3, s3 = stage(3)
-
-        @pl.when(live3)
-        def _():
-            relay(hidden.at[s3], h_send.at[s3], h_recv.at[s3])
-
-        live2, s2 = stage(2)
-
-        @pl.when(live2)
-        def _():
-            far_arrived(arrived.at[s2], x_send.at[s2], x_recv.at[s2])
-            rows = jnp.concatenate([arrived[s2, k] for k in range(n_tp)], axis=1)
-            gated = dot_nn(rows, w_gate[...])
-            up = dot_nn(rows, w_up[...])
-            hidden[s2, tp] = (gated * jax.nn.sigmoid(gated) * up).astype(BF16)
-            for copy in near_copies(hidden.at[s2], h_send.at[s2], h_recv.at[s2]):
-                copy.start()
-
-        live4, s4 = stage(4)
-
-        @pl.when(live4)
-        def _():
-            far_arrived(hidden.at[s4], h_send.at[s4], h_recv.at[s4])
-            rows = jnp.concatenate([hidden[s4, k] for k in range(n_tp)], axis=1)
-            block = dot_nn(rows, w_down[...]).astype(BF16)
-
-            @pl.when(i == 4)
+    blocks[plane] = normalise(rows, totals, gain[...], bias[...], features).astype(BF16)
+
+    def unit_plane(m):
+        return lax.rem(plane + toward * m + n_z, n_z)
+
+    def hop(u, to, slot):
+        return remote(
+            blocks.at[u], blocks.at[u], z_send.at[slot], z_recv.at[u], "sp", 2 * to + core
+        )
+
+    def z_round(d):
+        left, right = plane - d, plane + d
+
+        @pl.when(left >= 0)
+        def _():
+            hop(left, plane, left).wait_recv()
+
+            @pl.when(plane < n_z - 1)
             def _():
-                back[sp] = block
-
-            @pl.when(i > 4)
+                hop(left, plane + 1, left).start()
+
+        @pl.when(right < n_z)
+        def _():
+            hop(right, plane, right).wait_recv()
+
+            @pl.when(plane > 0)
             def _():
-                result[s4] = block
-                remote(
-                    result.at[s4], back.at[sp], r_send.at[s4], r_recv.at[sp], "sp", s4
-                ).start()
+                hop(right, plane - 1, right).start()
+
+    def aside_copy(i):
+        return remote(
+            aside.at[i], inputs.at[i, core, tp], a_send.at[i], a_recv.at[i], "tp", beside
+        )
+
+    def down_y(i, k, which):
+        ref = inputs.at[i, core, which]
+        return remote(ref, ref, y_send.at[i, k], y_recv.at[i, k], "tp", below)
+
+    def over(i, k, which, owner):
+        ref = inputs.at[i, owner, which]
+        return remote(ref, ref, d_send.at[i, k], d_recv.at[i, k], "sp", partner)
+
+    def pack(m):
+        u = unit_plane(m)
+        slot_rows = tables[u]
+        line = lax.broadcasted_iota(jnp.int32, (slots, positions), 0)
+
+        def pick(e):
+            mine = (line + e * slots).astype(F32)
+            hit = (mine == slot_rows[0:1]) | (mine == slot_rows[1:2])
+            return dot_nn(hit.astype(F32).astype(BF16), blocks[u]).astype(BF16)
+
+        away = pick(2 * plane + 1 - x)
+        for h in range(2):
+            aside[2 * m + h] = away[h * half : (h + 1) * half]
+            aside_copy(2 * m + h).start()
+        kept_rows = pick(expert)
+        for h in range(2):
+            i = 2 * m + h
+            inputs[i, core, tp] = kept_rows[h * half : (h + 1) * half]
+            down_y(i, 0, tp).start()
+            over(i, 0, tp, core).start()
+
+    def beside_arrived(i):
+        remote(
+            aside.at[i], inputs.at[i, core, beside], a_send.at[i], a_recv.at[i], "tp", beside
+        ).wait_recv()
+        down_y(i, 1, beside).start()
+        over(i, 1, beside, core).start()
+
+    def below_arrived(i):
+        for k, which in enumerate((below, far)):
+            down_y(i, k, which).wait_recv()
+            over(i, 2 + k, which, core).start()
+
+    quarter = 2 * y + core
+
+    def hidden_over(i, k, q):
+        ref = hidden.at[i, q]
+        return remote(ref, ref, h_send.at[i, k], h_recv.at[i, k], "sp", partner)
+
+    def hidden_down(i, q):
+        ref = hidden.at[i, q]
+        return remote(ref, ref, h_send.at[i, 1], h_recv.at[i, 1], "tp", below)
+
+    def expand(i):
+        for k, which in enumerate((tp, beside, below, far)):
+            over(i, k, which, 1 - core).wait_recv()
+        rows = jnp.concatenate(
+            [inputs[i, :, k].reshape(slots, part) for k in range(n_tp)], axis=1
+        )
+        gated = dot_nn(rows, w_gate[...])
+        up = dot_nn(rows, w_up[...])
+        hidden[i, quarter] = (gated * jax.nn.sigmoid(gated) * up).astype(BF16)
+        hidden_down(i, quarter).start()
+        hidden_over(i, 0, quarter).start()
+
+    q_partner = 2 * y + 1 - core
+    q_below = 2 * (1 - y) + core
+    q_far = 2 * (1 - y) + 1 - core
+
+    def is_own(i, c):
+        return (i < 2) & straight & (core == c)
+
+    def result_copy(i, c):
+        u = unit_plane(i // 2)
+        return remote_to(
+            result.at[i, c], back.at[expert, lax.rem(i, 2)], r_send.at[i, c],
+            r_recv.at[expert, lax.rem(i, 2)], {"sp": 2 * u + c, "tp": 2 * y + core},
+        )
+
+    def contract(i):
+        hidden_down(i, q_below).wait_recv()
+        hidden_over(i, 2, q_below).start()
+        hidden_over(i, 0, q_partner).wait_recv()
+        hidden_over(i, 2, q_far).wait_recv()
+        rows = jnp.concatenate([hidden[i, k] for k in range(n_tp)], axis=1)
+        block = dot_nn(rows, w_down[...]).astype(BF16)
+        for c in range(2):
+            result[i, c] = block[c * half : (c + 1) * half]
+
+            @pl.when(jnp.logical_not(is_own(i, c)))
+            def _():
+                result_copy(i, c).start()
+
+            @pl.when(is_own(i, c))
+            def _():
+                back[expert, lax.rem(i, 2)] = block[c * half : (c + 1) * half]
+
+    @pl.when(plane < n_z - 1)
+    def _():
+        hop(plane, plane + 1, plane).start()
+
+    @pl.when(plane > 0)
+    def _():
+        hop(plane, plane - 1, n_z).start()
+
+    pack(0)
+    cross(5, 8)
+    for d in range(1, n_z):
+        other = lax.rem(plane + d, n_z)
+        remote(
+            tables.at[other], tables.at[other], t_send.at[d], t_recv.at[other], "sp", partner
+        ).wait_recv()
+    beside_arrived(0)
+    beside_arrived(1)
+    z_round(1)
+    pack(1)
+    cross(8, 12)
+
+    def step(n, _):
+        s = lax.rem(n + 2, steps)
+        first = lax.rem(n, 2) == 0
+
+        @pl.when(first & (n < steps - 2))
+        def _():
+            beside_arrived(s)
+            beside_arrived(s + 1)
+
+        @pl.when(n == 0)
+        def _():
+            weights_here(0, 8)
+
+        @pl.when(n < steps)
+        def _():
+            below_arrived(s)
+            expand(s)
+
+        @pl.when(first & (n < steps - 4))
+        def _():
+            z_round(n // 2 + 2)
+            pack(n // 2 + 2)
+
+        @pl.when(n == 1)
+        def _():
+            weights_here(8, 12)
+
+        @pl.when(n > 0)
+        def _():
+            contract(lax.rem(n + 1, steps))
 
         return 0
 
-    lax.fori_loop(0, n_sp + 4, step, 0)
-    lane = lax.broadcasted_iota(jnp.int32, (positions, LANES), 1)
-    behind = (later < earlier).astype(F32).astype(BF16)
-    c0, c1 = columns[:, 1:2].astype(jnp.int32), columns[:, 2:3].astype(jnp.int32)
-    named = ((c0 == lane) | (c1 == lane)).astype(F32).astype(BF16)
-    rank = dot_nn(behind, named) + (lane * slots).astype(F32)
-    at0 = jnp.sum(jnp.where(c0 == lane, rank, 0.0), axis=1, keepdims=True).astype(jnp.int32)
-    at1 = jnp.sum(jnp.where(c1 == lane, rank, 0.0), axis=1, keepdims=True).astype(jnp.int32)
-    spot = lax.broadcasted_iota(jnp.int32, (positions, n_sp * slots), 1)
-    take0 = (spot == at0).astype(F32).astype(BF16)
-    take1 = (spot == at1).astype(F32).astype(BF16)
-    for k in range(1, n_sp):
-        s = lax.rem(sp + k, n_sp)
-        remote(result.at[s], back.at[s], r_send.at[s], r_recv.at[s], "sp", s).wait_recv()
-    returned = back[...].reshape(n_sp * slots, part)
-    moe = columns[:, 3:4] * dot_nn(take0, returned) + columns[:, 4:5] * dot_nn(take1, returned)
-    rows = ALPHA * normed[...].astype(F32) + moe
+    lax.fori_loop(0, steps + 1, step, 0)
+    at0, at1 = columns[:, 0:1], columns[:, 1:2]
+    spot = lax.broadcasted_iota(jnp.int32, (positions, 2 * slots), 1)
+    sum0 = jnp.zeros((positions, part), F32)
+    sum1 = jnp.zeros((positions, part), F32)
+    for d in range(1, n_z + 1):
+        u = lax.rem(plane + d, n_z)
+        for side in range(2):
+            e = 2 * u + side
+            local = (u == plane) & straight & (x == side)
+
+            @pl.when(jnp.logical_not(local))
+            def _():
+                for h in range(2):
+                    remote(
+                        result.at[0, 0], back.at[e, h], r_send.at[0, 0], r_recv.at[e, h],
+                        "sp", partner,
+                    ).wait_recv()
+
+        returned = back[pl.ds(2 * u, 2)].reshape(2 * slots, part)
+        spots = (spot + 2 * slots * u).astype(F32)
+        sum0 = sum0 + dot_nn((spots == at0).astype(F32).astype(BF16), returned)
+        sum1 = sum1 + dot_nn((spots == at1).astype(F32).astype(BF16), returned)
+    moe = columns[:, 3:4] * sum0 + columns[:, 4:5] * sum1
+    rows = ALPHA * blocks[plane].astype(F32) + moe
     totals = row_totals(rows, stats2, n_tp, stat2_send, stat2_recv)
     out[...] = normalise(rows, totals, gain2[...], bias2[...], features).astype(BF16)
 
     def drain(i, _):
-        s = lax.rem(sp + i, n_sp)
-
-        @pl.when(i > 0)
-        def _():
-            remote(packed.at[s], arrived.at[sp, tp], z_send.at[s], z_recv.at[sp], "sp", s).wait_send()
-            remote(result.at[s], back.at[sp], r_send.at[s], r_recv.at[sp], "sp", s).wait_send()
-
-        for buf, send, recv in ((arrived, x_send, x_recv), (hidden, h_send, h_recv)):
-            place = (buf.at[s], send.at[s], recv.at[s])
-            for copy in near_copies(*place) + relay_copies(*place):
-                copy.wait_send()
+        aside_copy(i).wait_send()
+        for k, which in enumerate((tp, beside)):
+            down_y(i, k, which).wait_send()
+        for k, which in enumerate((tp, beside, below, far)):
+            over(i, k, which, core).wait_send()
+        hidden_down(i, quarter).wait_send()
+        hidden_over(i, 0, quarter).wait_send()
+        hidden_over(i, 2, q_below).wait_send()
+        for c in range(2):
+            @pl.when(jnp.logical_not(is_own(i, c)))
+            def _():
+                result_copy(i, c).wait_send()
+
         return 0
 
-    lax.fori_loop(0, n_sp, drain, 0)
+    lax.fori_loop(0, steps, drain, 0)
+
+    @pl.when(jnp.logical_not(straight))
+    def _():
+        for copy in crossing:
+            copy.wait_send()
+
+    @pl.when(plane < n_z - 1)
+    def _():
+        hop(plane, plane + 1, plane).wait_send()
+        for d in range(1, n_z - 1):
+            @pl.when(plane - d >= 0)
+            def _():
+                hop(plane - d, plane + 1, plane - d).wait_send()
+
+    @pl.when(plane > 0)
+    def _():
+        hop(plane, plane - 1, n_z).wait_send()
+        for d in range(1, n_z - 1):
+            @pl.when(plane + d < n_z)
+            def _():
+                hop(plane + d, plane - 1, plane + d).wait_send()
+
+    for d in range(1, n_z):
+        table_copy(d).wait_send()
     edge.wait_send()
     edge_ids.wait_send()
     settle(tails, "sp", n_sp, tail_send, tail_recv)
@@ -545,12 +725,15 @@
     channels, positions = pool_in.shape
     part = residual.shape[1]
     pairs = routes.shape[1]
-    small = n_sp <= 16 and n_tp == 4 and pairs == 2
-    if not small or channels % LANES or positions % LANES or part % LANES:
+    slots = 2 * positions * pairs // n_sp
+    units = w_gate.shape[2]
+    small = n_sp in (8, 12, 16) and n_sp % 4 == 0 and n_tp == 4 and pairs == 2 and slots % 32 == 0
+    if not small or channels % LANES or positions % LANES or part % LANES or units % LANES:
         return general_body(*args)
     dma = pltpu.SemaphoreType.DMA
-    slots = 2 * positions * pairs // n_sp
-    units = w_gate.shape[2]
+    n_z = n_sp // 2
+    steps = 2 * n_z
+    half = slots // 2
     loaded = (w_out, gate_logit, residual, w_gate[0], w_up[0], w_down[0])
     vmem = pl.BlockSpec(memory_space=pltpu.VMEM)
     any_space = pl.BlockSpec(memory_space=pl.ANY)
@@ -567,17 +750,20 @@
             pltpu.VMEM((n_tp, positions, channels), BF16),
             pltpu.VMEM((n_tp, 8, positions), F32),
             pltpu.VMEM((n_tp, 8, positions), F32),
-            pltpu.VMEM((positions, part), BF16),
-            pltpu.VMEM((n_sp, slots, part), BF16),
-            pltpu.VMEM((n_sp, n_tp, slots, part), BF16),
-            pltpu.VMEM((n_sp, n_tp, slots, units), BF16),
-            pltpu.VMEM((n_sp, slots, part), BF16),
-            pltpu.VMEM((n_sp, slots, part), BF16),
-            dma((len(loaded),)),
+            pltpu.VMEM((n_z, 8, positions), F32),
+            pltpu.VMEM((n_z, positions, part), BF16),
+            pltpu.VMEM((steps, half, part), BF16),
+            pltpu.VMEM((steps, 2, n_tp, half, part), BF16),
+            pltpu.VMEM((steps, n_tp, slots, units), BF16),
+            pltpu.VMEM((steps, 2, half, part), BF16),
+            pltpu.VMEM((n_sp, 2, half, part), BF16),
+            dma((3,)), dma((12,)), dma((12,)),
             dma((2,)), dma((2,)), dma((n_sp,)), dma((n_sp,)),
             dma((n_tp,)), dma((n_tp,)), dma((n_tp,)), dma((n_tp,)),
-            dma((n_sp,)), dma((n_sp,)), dma((n_sp, 4)), dma((n_sp, 4)),
-            dma((n_sp, 4)), dma((n_sp, 4)), dma((n_sp,)), dma((n_sp,)),
+            dma((n_z,)), dma((n_z,)), dma((n_z + 1,)), dma((n_z,)),
+            dma((steps,)), dma((steps,)), dma((steps, 2)), dma((steps, 2)),
+            dma((steps, 4)), dma((steps, 4)), dma((steps, 3)), dma((steps, 3)),
+            dma((steps, 2)), dma((n_sp, 2)),
             dma((n_tp,)), dma((n_tp,)),
         ],
         compiler_params=pltpu.CompilerParams(

time: 127 us -> 121 us (0.953)
  the two profiles are of different devices: /device:TPU:25 before, /device:TPU:0 now
where the time goes in v1:
time: 121 us; the launch traced here: 120 us
  Pallas kernels  117 us (97%)
  local copies, waits for them, and re-layouts  3.01 us (2%)
    pallas_call x1, Pallas kernels, body(): pl.pallas_call(functools.partial(layer_kernel, n_sp, n_tp), out_shape=jax...  117 us
    unnamed x3, local copies, waits for them, and re-layouts  2.45 us

profile of v1, /device:TPU:0, one launch (start us, length us, event | category | flops | bytes accessed | tf_op | source)
XLA Modules:
  0.0 120.4 jit_solution(17080165791157746450)
XLA Ops:
  0.0 0.0 copy-start
  0.0 0.7 copy-done
  0.7 0.6 broadcast_in_dim.18.doc_row
  1.2 117.4 %shard_map.154 = bf16[384,512]{1,0:T(8,128)(2,1)} custom-call(bf16[128,384]{1,0:T(8,128)(2,1)} %pool.1, s32[1,384]{1,0:T(1,128)} %broadcast_in_dim.18.doc_row, s32[2,384]{1,0:T(2,128)} %bitcast.13, f32[2,384]{1,0:T(2,128)} %bitcast.14, bf16[8,64,64]{2,1,0:T(8,128)(2,1)} %pool_map.1, f32[1,512]{1,0:T(1,128)} %bitcast.15, f32[1,512]{1,0:T(1,128)} %bitcast.16, ...), custom_call_target="tpu_custom_call" | custom-call | tf_op jit(solution)/shard_map/pallas_call | solution.py:740
  118.6 1.8 %copy.18 = bf16[384,512]{1,0:T(8,128)(2,1)} copy(bf16[384,512]{1,0:T(8,128)(2,1)} %shard_map.154) | data formatting | bytes 786432
Async XLA Ops:
  0.0 0.7 copy-start

commit v2 on v1

--- a/solution.py
+++ b/solution.py
@@ -226,7 +226,7 @@
     return beside, lax.rem(tp + 2, 4), lax.rem(beside + 2, 4)
 
 
-def enter(n_sp):
+def greet(n_sp):
     sp = lax.axis_index("sp")
     beside, below, far = near_peers()
     barrier = pltpu.get_barrier_semaphore()
@@ -238,7 +238,10 @@
         )
     for peer in (below, far):
         pl.semaphore_signal(barrier, inc=1, device_id={"tp": peer})
-    pl.semaphore_wait(barrier, 2 * n_sp + 1)
+
+
+def all_here(n_sp):
+    pl.semaphore_wait(pltpu.get_barrier_semaphore(), 2 * n_sp + 1)
 
 
 def remote_to(src, dst, send, recv, device):
@@ -274,7 +277,7 @@
         ).wait_send()
 
 
-def row_totals(rows, stats, n_tp, send, recv):
+def row_totals(rows, stats, n_tp, send, recv, between=None):
     me = lax.axis_index("tp")
     lane = lax.broadcasted_iota(jnp.int32, (rows.shape[0], LANES), 1)
     first = jnp.sum(rows, axis=1, keepdims=True)
@@ -282,6 +285,8 @@
     both = jnp.where(lane == 0, first, jnp.where(lane == 1, second, 0.0))
     stats[me] = jnp.transpose(both)[:8]
     share(stats, "tp", n_tp, send, recv)
+    if between is not None:
+        between()
     collect(stats, "tp", n_tp, send, recv)
     total = stats[0]
     for k in range(1, n_tp):
@@ -298,10 +303,10 @@
 
 
 def layer_kernel(
-    n_sp, n_tp, pool, doc_row, route_row, weight_row, pool_map, scale, gain, bias, gain2, bias2,
+    n_sp, n_tp, pool, doc_ids, route_row, weight_row, pool_map, scale, gain, bias, gain2, bias2,
     w_out_hbm, gate_hbm, residual_hbm, w_gate_hbm, w_up_hbm, w_down_hbm, out,
     w_out, gate, residual, w_gate, w_up, w_down,
-    halo, halo_ids, tails, mapped, stats, stats2, tables, blocks,
+    doc_row, halo, halo_ids, tails, mapped, stats, stats2, tables, blocks,
     aside, inputs, hidden, result, back, load_sem, w_send, w_recv,
     halo_send, halo_recv, tail_send, tail_recv, map_send, map_recv, stat_send, stat_recv,
     t_send, t_recv, z_send, z_recv, a_send, a_recv, y_send, y_recv, d_send, d_recv,
@@ -320,6 +325,7 @@
     features = part * n_tp
     toward = 1 - 2 * (plane // (n_z // 2))
     straight = x == core
+    shift = jnp.where((plane > 0) & (plane < n_z - 1), 1, 0)
     expert = 2 * plane + x
     loads = [
         pltpu.make_async_copy(src, dst, load_sem.at[i])
@@ -330,7 +336,7 @@
     for load in loads:
         load.start()
     pieces = []
-    for pair, cuts in ((((w_gate_hbm, w_gate), (w_up_hbm, w_up)), 4), (((w_down_hbm, w_down),), 4)):
+    for pair, cuts in ((((w_gate_hbm, w_gate), (w_up_hbm, w_up)), 8), (((w_down_hbm, w_down),), 8)):
         for cut in range(cuts):
             for src, dst in pair:
                 size = dst.shape[0] // cuts
@@ -369,21 +375,14 @@
             for copy in crossing[first:last]:
                 copy.wait_recv()
 
-    enter(n_sp)
-    after = lax.rem(sp + 1, n_sp)
-    last = pl.ds(positions - LANES, LANES)
-    edge = remote(pool.at[:, last], halo, halo_send.at[0], halo_recv.at[0], "sp", after)
-    edge_ids = remote(doc_row.at[:, last], halo_ids, halo_send.at[1], halo_recv.at[1], "sp", after)
-    edge.start()
-    edge_ids.start()
-    cross(0, 3)
+    greet(n_sp)
+    doc_row[...] = doc_ids[...].reshape(1, positions)
     ids = doc_row[...].astype(F32)
     in_last = (ids == ids[:, positions - 1 :]).astype(F32)
     tail = dot_nt(jnp.broadcast_to(in_last, (8, positions)).astype(BF16), pool[...])
     kind = lax.broadcasted_iota(jnp.int32, tail.shape, 0)
     tail = jnp.where(kind == 1, jnp.sum(in_last, axis=1, keepdims=True), tail)
     tails[sp] = jnp.where(kind == 2, ids[:, positions - 1 :], tail)
-    share(tails, "sp", n_sp, tail_send, tail_recv)
     kind = lax.broadcasted_iota(jnp.int32, (LANES, positions), 0)
     later = lax.broadcasted_iota(jnp.int32, (positions, positions), 1)
     earlier = lax.broadcasted_iota(jnp.int32, (positions, positions), 0)
@@ -404,12 +403,21 @@
             tables.at[plane], tables.at[plane], t_send.at[d], t_recv.at[plane], "sp", 2 * to + core
         )
 
-    for d in range(1, n_z):
-        table_copy(d).start()
     columns = jnp.transpose(table)
     col = columns[:, 2:3]
     place = lax.broadcasted_iota(jnp.int32, (positions, LANES + positions), 1) - LANES
     delta = lax.broadcasted_iota(jnp.int32, (positions, LANES + positions), 0) - place
+    all_here(n_sp)
+    after = lax.rem(sp + 1, n_sp)
+    last = pl.ds(positions - LANES, LANES)
+    edge = remote(pool.at[:, last], halo, halo_send.at[0], halo_recv.at[0], "sp", after)
+    edge_ids = remote(doc_row.at[:, last], halo_ids, halo_send.at[1], halo_recv.at[1], "sp", after)
+    edge.start()
+    edge_ids.start()
+    share(tails, "sp", n_sp, tail_send, tail_recv)
+    cross(0, 5)
+    for d in range(1, n_z):
+        table_copy(d).start()
     edge.wait_recv()
     edge_ids.wait_recv()
     ext = jnp.concatenate([halo[...], pool[...]], axis=1)
@@ -450,7 +458,7 @@
         factor = scale[:, pl.ds(pl.multiple_of(tp * channels, LANES), channels)][:, span]
         mapped[tp, :, span] = (dot_nn(pooled, pool_map[group]) * factor).astype(BF16)
     share(mapped, "tp", n_tp, map_send, map_recv)
-    cross(3, 5)
+    cross(5, 7)
     for load in loads:
         load.wait()
     opened = jax.nn.sigmoid(gate[...].astype(F32))
@@ -458,11 +466,14 @@
     collect(mapped, "tp", n_tp, map_send, map_recv)
     every = jnp.concatenate([mapped[k] for k in range(n_tp)], axis=1)
     rows = kept + dot_nn(every, w_out[...]) * opened
-    totals = row_totals(rows, stats, n_tp, stat_send, stat_recv)
+    totals = row_totals(rows, stats, n_tp, stat_send, stat_recv, lambda: cross(7, 11))
     blocks[plane] = normalise(rows, totals, gain[...], bias[...], features).astype(BF16)
 
     def unit_plane(m):
-        return lax.rem(plane + toward * m + n_z, n_z)
+        return lax.rem(plane + toward * (m + shift) + 2 * n_z, n_z)
+
+    def packed_unit(p):
+        return lax.rem(p - shift + n_z, n_z)
 
     def hop(u, to, slot):
         return remote(
@@ -561,7 +572,7 @@
     q_far = 2 * (1 - y) + 1 - core
 
     def is_own(i, c):
-        return (i < 2) & straight & (core == c)
+        return (unit_plane(i // 2) == plane) & straight & (core == c)
 
     def result_copy(i, c):
         u = unit_plane(i // 2)
@@ -570,9 +581,11 @@
             r_recv.at[expert, lax.rem(i, 2)], {"sp": 2 * u + c, "tp": 2 * y + core},
         )
 
-    def contract(i):
+    def below_hidden(i):
         hidden_down(i, q_below).wait_recv()
         hidden_over(i, 2, q_below).start()
+
+    def contract(i):
         hidden_over(i, 0, q_partner).wait_recv()
         hidden_over(i, 2, q_far).wait_recv()
         rows = jnp.concatenate([hidden[i, k] for k in range(n_tp)], axis=1)
@@ -596,59 +609,86 @@
     def _():
         hop(plane, plane - 1, n_z).start()
 
-    pack(0)
-    cross(5, 8)
+    pack(packed_unit(0))
+    cross(11, 16)
     for d in range(1, n_z):
         other = lax.rem(plane + d, n_z)
         remote(
             tables.at[other], tables.at[other], t_send.at[d], t_recv.at[other], "sp", partner
         ).wait_recv()
-    beside_arrived(0)
-    beside_arrived(1)
+
+    def both_beside(p):
+        i = 2 * packed_unit(p)
+        beside_arrived(i)
+        beside_arrived(i + 1)
+
+    both_beside(0)
     z_round(1)
-    pack(1)
-    cross(8, 12)
-
-    def step(n, _):
-        s = lax.rem(n + 2, steps)
-        first = lax.rem(n, 2) == 0
-
-        @pl.when(first & (n < steps - 2))
-        def _():
-            beside_arrived(s)
-            beside_arrived(s + 1)
-
-        @pl.when(n == 0)
-        def _():
-            weights_here(0, 8)
-
-        @pl.when(n < steps)
-        def _():
-            below_arrived(s)
-            expand(s)
-
-        @pl.when(first & (n < steps - 4))
-        def _():
-            z_round(n // 2 + 2)
-            pack(n // 2 + 2)
-
-        @pl.when(n == 1)
-        def _():
-            weights_here(8, 12)
-
-        @pl.when(n > 0)
-        def _():
-            contract(lax.rem(n + 1, steps))
+    pack(packed_unit(1))
+    cross(16, 20)
+
+    def step(p, _):
+        @pl.when(p + 1 < n_z)
+        def _():
+            both_beside(p + 1)
+
+        @pl.when(p + 2 < n_z)
+        def _():
+            z_round(p + 2)
+            pack(packed_unit(p + 2))
+
+        @pl.when(p == 0)
+        def _():
+            cross(20, 24)
+
+        @pl.when(p == 1)
+        def _():
+            cross(24, 24)
+
+        @pl.when(p > 0)
+        def _():
+            below_hidden(2 * p - 2)
+
+        @pl.when(p > 0)
+        def _():
+            below_hidden(2 * p - 1)
+
+        @pl.when(p == 1)
+        def _():
+            weights_here(16, 24)
+
+        @pl.when(p > 0)
+        def _():
+            contract(2 * p - 2)
+
+        @pl.when(p > 0)
+        def _():
+            contract(2 * p - 1)
+
+        @pl.when(p == 0)
+        def _():
+            weights_here(0, 16)
+
+        @pl.when(p < n_z)
+        def _():
+            below_arrived(2 * p + 0)
+            expand(2 * p + 0)
+
+        @pl.when(p < n_z)
+        def _():
+            below_arrived(2 * p + 1)
+            expand(2 * p + 1)
 
         return 0
 
-    lax.fori_loop(0, steps + 1, step, 0)
+    lax.fori_loop(0, n_z + 1, step, 0)
     at0, at1 = columns[:, 0:1], columns[:, 1:2]
     spot = lax.broadcasted_iota(jnp.int32, (positions, 2 * slots), 1)
     sum0 = jnp.zeros((positions, part), F32)
     sum1 = jnp.zeros((positions, part), F32)
-    for d in range(1, n_z + 1):
-        u = lax.rem(plane + d, n_z)
+    inner = jnp.where((plane > 0) & (plane < n_z - 1), 1, 0)
+    for d in range(n_z):
+        u = lax.rem(plane + toward * (d + inner) + 2 * n_z, n_z)
         for side in range(2):
             e = 2 * u + side
             local = (u == plane) & straight & (x == side)
@@ -727,7 +767,7 @@
     pairs = routes.shape[1]
     slots = 2 * positions * pairs // n_sp
     units = w_gate.shape[2]
-    small = n_sp in (8, 12, 16) and n_sp % 4 == 0 and n_tp == 4 and pairs == 2 and slots % 32 == 0
+    small = n_sp == 8 and n_tp == 4 and pairs == 2 and slots % 32 == 0
     if not small or channels % LANES or positions % LANES or part % LANES or units % LANES:
         return general_body(*args)
     dma = pltpu.SemaphoreType.DMA
@@ -744,6 +784,7 @@
         out_specs=vmem,
         scratch_shapes=[
             *(pltpu.VMEM(x.shape, x.dtype) for x in loaded),
+            pltpu.VMEM((1, positions), jnp.int32),
             pltpu.VMEM((channels, LANES), BF16),
             pltpu.VMEM((1, LANES), jnp.int32),
             pltpu.VMEM((n_sp, 8, channels), F32),
@@ -757,7 +798,7 @@
             pltpu.VMEM((steps, n_tp, slots, units), BF16),
             pltpu.VMEM((steps, 2, half, part), BF16),
             pltpu.VMEM((n_sp, 2, half, part), BF16),
-            dma((3,)), dma((12,)), dma((12,)),
+            dma((3,)), dma((24,)), dma((24,)),
             dma((2,)), dma((2,)), dma((n_sp,)), dma((n_sp,)),
             dma((n_tp,)), dma((n_tp,)), dma((n_tp,)), dma((n_tp,)),
             dma((n_z,)), dma((n_z,)), dma((n_z + 1,)), dma((n_z,)),
@@ -770,7 +811,7 @@
             collective_id=0, has_side_effects=True, vmem_limit_bytes=60 << 20
         ),
     )(
-        pool_in, doc_ids[None], routes.T, route_weight.T, pool_map, pool_scale[None],
+        pool_in, doc_ids, routes.T, route_weight.T, pool_map, pool_scale[None],
         first_gain[None], first_bias[None], second_gain[None], second_bias[None], *loaded,
     )
 

time: 121 us -> 110 us (0.909)
  Pallas kernels: 117 us -> 108 us
  local copies, waits for them, and re-layouts: 3.01 us -> 1.77 us
    pallas_call x1, Pallas kernels: 117 us -> 108 us  [body(): pl.pallas_call(functools.partial(layer_kernel, n_sp, n_tp), out_shape=jax...]
    unnamed x3 -> x1, local copies, waits for them, and re-layouts: 2.45 us -> 1.77 us
where the time goes in v2:
time: 110 us
  Pallas kernels  108 us (98%)
  local copies, waits for them, and re-layouts  1.77 us (2%)
    pallas_call x1, Pallas kernels, body(): pl.pallas_call(functools.partial(layer_kernel, n_sp, n_tp), out_shape=jax...  108 us

profile of v2, /device:TPU:0, one launch (start us, length us, event | category | flops | bytes accessed | tf_op | source)
XLA Modules:
  0.0 109.6 jit_solution(13609790304177137658)
XLA Ops:
  0.0 107.9 %shard_map.154 = bf16[384,512]{1,0:T(8,128)(2,1)} custom-call(bf16[128,384]{1,0:T(8,128)(2,1)} %pool.1, s32[384]{0:T(512)} %doc_ids.1, s32[2,384]{1,0:T(2,128)} %bitcast.13, f32[2,384]{1,0:T(2,128)} %bitcast.14, bf16[8,64,64]{2,1,0:T(8,128)(2,1)} %pool_map.1, f32[1,512]{1,0:T(1,128)} %bitcast.15, f32[1,512]{1,0:T(1,128)} %bitcast.16, f32[1,512]{1,0:T(1,128)} %bitcast.17, ...), custom_call_target="tpu_custom_call" | custom-call | tf_op jit(solution)/shard_map/pallas_call | solution.py:780
  107.9 1.8 %copy.18 = bf16[384,512]{1,0:T(8,128)(2,1)} copy(bf16[384,512]{1,0:T(8,128)(2,1)} %shard_map.154) | data formatting | bytes 786432

commit v3 on v2

--- a/solution.py
+++ b/solution.py
@@ -307,9 +307,9 @@
     w_out_hbm, gate_hbm, residual_hbm, w_gate_hbm, w_up_hbm, w_down_hbm, out,
     w_out, gate, residual, w_gate, w_up, w_down,
     doc_row, halo, halo_ids, tails, mapped, stats, stats2, tables, blocks,
-    aside, inputs, hidden, result, back, load_sem, w_send, w_recv,
+    aside, passing, inputs, hidden, result, back, load_sem, w_send, w_recv,
     halo_send, halo_recv, tail_send, tail_recv, map_send, map_recv, stat_send, stat_recv,
-    t_send, t_recv, z_send, z_recv, a_send, a_recv, y_send, y_recv, d_send, d_recv,
+    t_send, t_recv, z_send, z_recv, a_send, a_recv, p_send, p_recv, y_send, y_recv, d_send, d_recv,
     h_send, h_recv, r_send, r_recv, stat2_send, stat2_recv,
 ):
     sp, tp = lax.axis_index("sp"), lax.axis_index("tp")
@@ -504,6 +504,15 @@
             aside.at[i], inputs.at[i, core, tp], a_send.at[i], a_recv.at[i], "tp", beside
         )
 
+    def aside_over(i):
+        return remote(aside.at[i], passing.at[i], a_send.at[i], p_recv.at[i], "sp", partner)
+
+    def aside_pass(i):
+        return remote_to(
+            passing.at[i], inputs.at[i, 1 - core, tp], p_send.at[i], a_recv.at[i],
+            {"sp": partner, "tp": beside},
+        )
+
     def down_y(i, k, which):
         ref = inputs.at[i, core, which]
         return remote(ref, ref, y_send.at[i, k], y_recv.at[i, k], "tp", below)
@@ -525,13 +534,28 @@
         away = pick(2 * plane + 1 - x)
         for h in range(2):
             aside[2 * m + h] = away[h * half : (h + 1) * half]
-            aside_copy(2 * m + h).start()
+            i = 2 * m + h
+
+            @pl.when(straight)
+            def _():
+                aside_copy(i).start()
+
+            @pl.when(jnp.logical_not(straight))
+            def _():
+                aside_over(i).start()
+
         kept_rows = pick(expert)
         for h in range(2):
             i = 2 * m + h
             inputs[i, core, tp] = kept_rows[h * half : (h + 1) * half]
             down_y(i, 0, tp).start()
             over(i, 0, tp, core).start()
+
+        @pl.when(straight)
+        def _():
+            for h in range(2):
+                aside_over(2 * m + h).wait_recv()
+                aside_pass(2 * m + h).start()
 
     def beside_arrived(i):
         remote(
@@ -712,6 +736,11 @@
 
     def drain(i, _):
         aside_copy(i).wait_send()
+
+        @pl.when(straight)
+        def _():
+            aside_pass(i).wait_send()
+
         for k, which in enumerate((tp, beside)):
             down_y(i, k, which).wait_send()
         for k, which in enumerate((tp, beside, below, far)):
@@ -794,6 +823,7 @@
             pltpu.VMEM((n_z, 8, positions), F32),
             pltpu.VMEM((n_z, positions, part), BF16),
             pltpu.VMEM((steps, half, part), BF16),
+            pltpu.VMEM((steps, half, part), BF16),
             pltpu.VMEM((steps, 2, n_tp, half, part), BF16),
             pltpu.VMEM((steps, n_tp, slots, units), BF16),
             pltpu.VMEM((steps, 2, half, part), BF16),
@@ -802,7 +832,7 @@
             dma((2,)), dma((2,)), dma((n_sp,)), dma((n_sp,)),
             dma((n_tp,)), dma((n_tp,)), dma((n_tp,)), dma((n_tp,)),
             dma((n_z,)), dma((n_z,)), dma((n_z + 1,)), dma((n_z,)),
-            dma((steps,)), dma((steps,)), dma((steps, 2)), dma((steps, 2)),
+            dma((steps,)), dma((steps,)), dma((steps,)), dma((steps,)), dma((steps, 2)), dma((steps, 2)),
             dma((steps, 4)), dma((steps, 4)), dma((steps, 3)), dma((steps, 3)),
             dma((steps, 2)), dma((n_sp, 2)),
             dma((n_tp,)), dma((n_tp,)),

time: 110 us -> 109 us (level)
  no operation moved by 1% of the time
where the time goes in v3:
time: 109 us
  Pallas kernels  107 us (98%)
  local copies, waits for them, and re-layouts  1.77 us (2%)
    pallas_call x1, Pallas kernels, body(): pl.pallas_call(functools.partial(layer_kernel, n_sp, n_tp), out_shape=jax...  107 us

profile of v3, /device:TPU:0, one launch (start us, length us, event | category | flops | bytes accessed | tf_op | source)
XLA Modules:
  0.0 108.6 jit_solution(4955181837039919510)
XLA Ops:
  0.0 106.8 %shard_map.154 = bf16[384,512]{1,0:T(8,128)(2,1)} custom-call(bf16[128,384]{1,0:T(8,128)(2,1)} %pool.1, s32[384]{0:T(512)} %doc_ids.1, s32[2,384]{1,0:T(2,128)} %bitcast.13, f32[2,384]{1,0:T(2,128)} %bitcast.14, bf16[8,64,64]{2,1,0:T(8,128)(2,1)} %pool_map.1, f32[1,512]{1,0:T(1,128)} %bitcast.15, f32[1,512]{1,0:T(1,128)} %bitcast.16, f32[1,512]{1,0:T(1,128)} %bitcast.17, ...), custom_call_target="tpu_custom_call" | custom-call | tf_op jit(solution)/shard_map/pallas_call | solution.py:809
  106.8 1.8 %copy.18 = bf16[384,512]{1,0:T(8,128)(2,1)} copy(bf16[384,512]{1,0:T(8,128)(2,1)} %shard_map.154) | data formatting | bytes 786432
